TPU v7x, 512 devices: a whole 4x8x8 slice. The times are simulated.
512 devices in a mesh: kv: 64 (over z, y), tp: 8 (over x, core).
Axes of the slice: x: 4, y: 8, z: 8, core: 2. Of those that a mesh axis runs over, the one named last changes fastest.
Arguments:
- queries: bfloat16 [8192, 1024], P('kv', 'tp'), may hold values from -4 to 4
- keys: bfloat16 [8192, 1024], P('kv', 'tp'), may hold values from -4 to 4
- values: bfloat16 [8192, 1024], P('kv', 'tp'), may hold values from -4 to 4
- cotangent: bfloat16 [8192, 1024], P('kv', 'tp'), may hold values from -4 to 4
- log_sum: float32 [16, 8192], P('tp', 'kv'), may hold values from 4.5 to 7.5
- chosen: int32 [16, 256, 12], P('tp'), may hold values from 0 to 255, as said below
- normed_input: bfloat16 [8192, 2048], P('kv', 'tp'), may hold values from -0.0625 to 0.0625
Outputs:
- grad_queries: bfloat16 [8192, 1024], P('kv', 'tp')
- grad_keys: bfloat16 [8192, 1024], P('kv', 'tp')
- grad_values: bfloat16 [8192, 1024], P('kv', 'tp')
- grad_weight: float32 [2048, 1024], P('kv', 'tp')
Inputs may be any that keep to these rules, and one draw needn't show every extreme that they name: `chosen`: for each head, the distinct blocks below their own query block that the query blocks of one device's 128 positions choose include at most 1 block of any one device's span of 128 positions, and exactly 1 for some pairs of devices. Within one list the entries below the query block's own index are distinct.
All inputs are finite; a program needn't handle non-finite values.
Results may differ from a plain program's by a relative error of at most 0.0085.
Values may be sent and summed in bfloat16 or wider, within the bound.
No kernel may reach another device: no remote copies, remote signals or barrier semaphores. Data moves between devices by JAX's collectives and lax.ppermute only.
A program may use at most 64 MiB of HBM per device.

v0:
```python
import jax
import jax.numpy as jnp
from jax import lax
from jax.sharding import PartitionSpec as P

HD = 64
BLK = 32
SEL = 12
MOST = 1


MASKED = -1e30


def sent_together(arrays, axis, split_dim, concat_dim, along):
    both = jnp.concatenate(arrays, axis=along)
    whole, at, finished = (
        lax.all_to_all(both, axis, split_axis=split_dim, concat_axis=concat_dim, tiled=True),
        0,
        [],
    )
    for a in arrays:
        finished.append(lax.slice_in_dim(whole, at, at + a.shape[along], axis=along))
        at += a.shape[along]
    return tuple(finished)


def split_up(array, dim, size):
    dims = array.shape
    tiles = array.reshape(*dims[:dim], size, dims[dim] // size, *dims[dim + 1 :])
    return jnp.moveaxis(tiles, dim, 0)


def sum_at_owner(array, axis, dim):
    tiles = split_up(array, dim, lax.axis_size(axis))
    arrived = lax.all_to_all(tiles, axis, split_axis=0, concat_axis=0, tiled=True)
    return arrived.astype(jnp.float32).sum(axis=0)


def slot_picks(needed):
    span_width = needed.shape[-1]
    counted = needed.astype(jnp.int32)
    before = jnp.cumsum(counted, axis=-1) - counted
    places = jnp.arange(span_width, dtype=jnp.int32)
    picked, present = ([], [])
    hitting = needed & (before == 0)
    present.append(jnp.any(hitting, axis=-1))
    picked.append(jnp.sum(jnp.where(hitting, places, 0), axis=-1))
    return (jnp.stack(picked, axis=-1), jnp.stack(present, axis=-1))


def to_blocks(row_block, tok_rows, head_count):
    shards = row_block.shape[0] // tok_rows
    shaped = row_block.reshape(shards, tok_rows // BLK, BLK, head_count, HD).transpose(
        0, 3, 1, 2, 4
    )
    return shaped.reshape(shards * head_count * (tok_rows // BLK), BLK * HD)


def heads_from(row_block, head_count):
    blocks_dev = row_block.shape[0] // BLK
    return row_block.reshape(blocks_dev, BLK, head_count, HD).transpose(2, 0, 1, 3)


def back_rows(blocked):
    head_count, blocks_dev = (blocked.shape[0], blocked.shape[1])
    return blocked.transpose(1, 2, 0, 3).reshape(blocks_dev * BLK, head_count * HD)


def body(queries, keys, values, cotangent, log_sum, chosen, normed_input):
    tok_rows = queries.shape[0]
    head_count = log_sum.shape[0]
    blocks_dev = tok_rows // BLK
    devices = lax.axis_size("kv")
    my_index = lax.axis_index("kv")
    block_total = chosen.shape[1]
    tile_size = BLK * HD
    score_scale = HD ** (-0.5)
    places = jnp.arange(blocks_dev, dtype=jnp.int32)
    own_ids = my_index * blocks_dev + places
    my_lists = lax.dynamic_slice_in_dim(chosen, my_index * blocks_dev, blocks_dev, 1)
    usable = my_lists < own_ids[None, :, None]
    every_block = jnp.arange(block_total, dtype=jnp.int32)
    need_here = jnp.any((my_lists[..., None] == every_block) & usable[..., None], axis=(1, 2))
    req_picked, req_present = slot_picks(need_here.reshape(head_count, devices, blocks_dev))
    grouped = chosen.reshape(head_count, devices, blocks_dev, SEL)
    row_ids = every_block.reshape(devices, blocks_dev)
    usable_all = grouped < row_ids[None, :, :, None]
    need_there = jnp.any((grouped[..., None] == own_ids) & usable_all[..., None], axis=(2, 3))
    own_picked, own_present = slot_picks(need_there)
    own_picked = own_picked.transpose(1, 0, 2)
    own_present = own_present.transpose(1, 0, 2)
    head_base = (jnp.arange(head_count, dtype=jnp.int32) * blocks_dev)[None, :, None]
    send_ids = (head_base + own_picked).reshape(-1)
    key_send = jnp.take(to_blocks(keys, tok_rows, head_count), send_ids, axis=0).reshape(
        devices, head_count, MOST, tile_size
    )
    value_send = jnp.take(to_blocks(values, tok_rows, head_count), send_ids, axis=0).reshape(
        devices, head_count, MOST, tile_size
    )
    key_tiles, value_tiles = sent_together((key_send, value_send), "kv", 0, 0, 1)
    owners = my_lists // blocks_dev
    local_ids = my_lists % blocks_dev
    head_ids = jnp.arange(head_count, dtype=jnp.int32)[:, None, None]
    rows_at = (head_ids * devices + owners).reshape(-1)
    slot_at = jnp.take(req_picked.reshape(head_count * devices, MOST), rows_at, axis=0).reshape(
        head_count, blocks_dev, SEL, MOST
    )
    slot_live = jnp.take(req_present.reshape(head_count * devices, MOST), rows_at, axis=0).reshape(
        head_count, blocks_dev, SEL, MOST
    )
    matches = (slot_at == local_ids[..., None]) & slot_live
    slot_of = jnp.sum(jnp.where(matches, jnp.arange(MOST, dtype=jnp.int32), 0), axis=-1)
    tile_ids = jnp.where(usable, (owners * head_count + head_ids) * MOST + slot_of, 0).reshape(-1)
    sel_keys = jnp.take(key_tiles.reshape(-1, tile_size), tile_ids, axis=0).reshape(
        head_count, blocks_dev, SEL * BLK, HD
    )
    sel_values = jnp.take(value_tiles.reshape(-1, tile_size), tile_ids, axis=0).reshape(
        head_count, blocks_dev, SEL * BLK, HD
    )
    keys_all = jnp.concatenate([sel_keys, heads_from(keys, head_count)], axis=2)
    values_all = jnp.concatenate([sel_values, heads_from(values, head_count)], axis=2)
    causal = jnp.arange(BLK)[:, None] >= jnp.arange(BLK)[None, :]
    sel_mask = jnp.broadcast_to(
        jnp.repeat(usable, BLK, axis=2)[:, :, None, :], (head_count, blocks_dev, BLK, SEL * BLK)
    )
    allowed = jnp.concatenate(
        [sel_mask, jnp.broadcast_to(causal, (head_count, blocks_dev, BLK, BLK))], axis=3
    )
    q_blocks = heads_from(queries, head_count)
    g_blocks = heads_from(cotangent, head_count)
    log_rows = log_sum.reshape(head_count, blocks_dev, BLK)[..., None]
    scores = (
        jnp.einsum("hiqd,hikd->hiqk", q_blocks, keys_all, preferred_element_type=jnp.float32)
        * score_scale
    )
    weights = jnp.exp(jnp.where(allowed, scores - log_rows, MASKED))
    value_dots = jnp.einsum(
        "hiqd,hikd->hiqk", g_blocks, values_all, preferred_element_type=jnp.float32
    )
    row_delta = jnp.sum(weights * value_dots, axis=-1, keepdims=True)
    score_grad = (weights * (value_dots - row_delta)).astype(jnp.bfloat16)
    weights_low = weights.astype(jnp.bfloat16)
    query_grad = (
        jnp.einsum("hiqk,hikd->hiqd", score_grad, keys_all, preferred_element_type=jnp.float32)
        * score_scale
    )
    key_grad = (
        jnp.einsum("hiqk,hiqd->hikd", score_grad, q_blocks, preferred_element_type=jnp.float32)
        * score_scale
    )
    value_grad = jnp.einsum(
        "hiqk,hiqd->hikd", weights_low, g_blocks, preferred_element_type=jnp.float32
    )
    grad_queries = back_rows(query_grad).astype(jnp.bfloat16)

    def to_slots(gradient):
        chosen_part = gradient[:, :, : SEL * BLK].reshape(-1, tile_size)
        slotted = jax.ops.segment_sum(
            chosen_part, tile_ids, num_segments=devices * head_count * MOST
        )
        return slotted.reshape(devices, head_count, MOST, tile_size)

    back_keys, back_values = (
        lax.all_to_all(
            to_slots(key_grad).astype(jnp.bfloat16), "kv", split_axis=0, concat_axis=0, tiled=True
        ).astype(jnp.float32),
        lax.all_to_all(
            to_slots(value_grad).astype(jnp.bfloat16), "kv", split_axis=0, concat_axis=0, tiled=True
        ).astype(jnp.float32),
    )
    land_ids = jnp.where(own_present, head_base + own_picked, head_count * blocks_dev).reshape(-1)

    def settle(returned, gradient):
        flat_tiles = returned.reshape(-1, tile_size)
        targets = (
            jnp.arange(head_count * blocks_dev, dtype=jnp.int32)[:, None] == land_ids[None, :]
        ).astype(jnp.float32)
        landed = jnp.dot(
            targets, flat_tiles, precision=lax.Precision.HIGHEST, preferred_element_type=jnp.float32
        )
        summed = landed.reshape(head_count, blocks_dev, BLK, HD) + gradient[:, :, SEL * BLK :]
        return back_rows(summed).astype(jnp.bfloat16)

    grad_keys = settle(back_keys, key_grad)
    grad_values = settle(back_values, value_grad)
    whole_input = lax.all_gather(normed_input, "tp", axis=1, tiled=True)
    grad_weight = sum_at_owner(
        lax.dot_general(
            whole_input, grad_queries, (((0,), (0,)), ((), ())), preferred_element_type=jnp.float32
        ).astype(jnp.bfloat16),
        "kv",
        0,
    )
    return (grad_queries, grad_keys, grad_values, grad_weight)


def solution(mesh):
    in_specs = (
        P("kv", "tp"),
        P("kv", "tp"),
        P("kv", "tp"),
        P("kv", "tp"),
        P("tp", "kv"),
        P("tp", None, None),
        P("kv", "tp"),
    )
    out_specs = (P("kv", "tp"), P("kv", "tp"), P("kv", "tp"), P("kv", "tp"))
    return jax.shard_map(body, mesh=mesh, in_specs=in_specs, out_specs=out_specs, check_vma=False)
```

profile of v0, /device:TPU:8, one launch (start us, length us, event | category | flops | bytes accessed | tf_op | source)
XLA Modules:
  0.0 145.6 jit_solution(14934738471255190425)
XLA Ops:
  0.7 0.9 copy.75
  2.6 0.8 reshape.213
  3.9 0.9 gather_fusion
  4.8 0.9 gather_fusion.1
  6.0 0.3 reshape.219
  6.3 0.3 reshape.216
  6.6 2.1 %pad_maximum_fusion = bf16[64,4,1,2048]{3,1,2,0:T(4,128)(2,1)} fusion(bf16[64,2,1,2048]{3,1,2,0:T(2,128)(2,1)S(1)} %bitcast.101, bf16[64,2,1,2048]{3,1,2,0:T(2,128)(2,1)S(1)} %bitcast.102), kind=kLoop, calls=%fused_computation.18 | loop fusion | flops 2097152 | bytes 2097152 | tf_op jit(solution)/shard_map/concatenate | solution.py:16
  8.7 16.7 %all-to-all-start = ((bf16[64,4,1,2048]{3,1,2,0:T(4,128)(2,1)}), bf16[64,4,1,2048]{3,1,2,0:T(4,128)(2,1)S(1)}, u32[]{:S(2)}, u32[]{:S(2)}) async-start(bf16[64,4,1,2048]{3,1,2,0:T(4,128)(2,1)} %pad_maximum_fusion), calls=%async_computation | async-start | bytes 2097152 | tf_op jit(solution)/shard_map/all_to_all | solution.py:18
  26.9 27.8 %all-to-all-done = bf16[64,4,1,2048]{3,1,2,0:T(4,128)(2,1)S(1)} async-done(((bf16[64,4,1,2048]{3,1,2,0:T(4,128)(2,1)}), bf16[64,4,1,2048]{3,1,2,0:T(4,128)(2,1)S(1)}, u32[]{:S(2)}, u32[]{:S(2)}) %all-to-all-start) | async-done | bytes 1048608 | tf_op jit(solution)/shard_map/all_to_all | solution.py:18
  54.7 0.7 fusion.46
  55.9 0.8 gather_fusion.3
  56.7 0.8 gather_fusion.2
  57.7 0.8 reshape.226
  58.5 0.3 copy.87
  58.8 0.8 reshape.222
  59.6 0.3 copy.84
  60.2 0.4 multiply_reduce_fusion
  60.8 0.3 convolution_multiply_fusion
  61.2 0.3 copy-done.1
  61.7 0.5 copy.91
  62.1 0.5 reshape.270
  62.6 2.0 %scatter_custom_fusion = f32[128,2048]{1,0:T(8,128)S(1)} fusion(s32[96]{0:T(128)S(1)} %reshape.221, f32[96,2048]{1,0:T(8,128)S(1)} %reshape.270, f32[]{:T(128)} %constant.105.clone.1), kind=kCustom, calls=%fused_computation.26 | custom fusion | flops 196608 | bytes 1048580 | tf_op jit(solution)/shard_map/scatter-add | solution.py:159
  64.7 1.2 convert_element_type.84
  65.9 7.1 %all-to-all-start.1 = ((bf16[64,2,1,2048]{3,1,2,0:T(2,128)(2,1)}), bf16[64,2,1,2048]{3,1,2,0:T(2,128)(2,1)}, u32[]{:S(2)}, u32[]{:S(2)}) async-start(bf16[64,2,1,2048]{3,1,2,0:T(2,128)(2,1)} %bitcast.18), calls=%async_computation.1 | async-start | bytes 1048576 | tf_op jit(solution)/shard_map/all_to_all | solution.py:165
  73.1 0.3 fusion.16
  73.4 1.0 copy-done
  74.4 0.5 copy.96
  74.9 0.5 reshape.278
  75.4 2.0 %scatter_custom_fusion.1 = f32[128,2048]{1,0:T(8,128)S(1)} fusion(s32[96]{0:T(128)S(1)} %reshape.221, f32[96,2048]{1,0:T(8,128)S(1)} %reshape.278, f32[]{:T(128)} %constant.105.clone.1), kind=kCustom, calls=%fused_computation.24 | custom fusion | flops 196608 | bytes 1048580 | tf_op jit(solution)/shard_map/scatter-add | solution.py:159
  77.6 1.1 convert_element_type.90
  78.7 12.8 %all-to-all-done.1 = bf16[64,2,1,2048]{3,1,2,0:T(2,128)(2,1)} async-done(((bf16[64,2,1,2048]{3,1,2,0:T(2,128)(2,1)}), bf16[64,2,1,2048]{3,1,2,0:T(2,128)(2,1)}, u32[]{:S(2)}, u32[]{:S(2)}) %all-to-all-start.1) | async-done | bytes 524320 | tf_op jit(solution)/shard_map/all_to_all | solution.py:165
  91.5 5.4 %all-to-all-start.2 = ((bf16[64,2,1,2048]{3,1,2,0:T(2,128)(2,1)}), bf16[64,2,1,2048]{3,1,2,0:T(2,128)(2,1)S(1)}, u32[]{:S(2)}, u32[]{:S(2)}) async-start(bf16[64,2,1,2048]{3,1,2,0:T(2,128)(2,1)} %bitcast.24), calls=%async_computation.2 | async-start | bytes 1048576 | tf_op jit(solution)/shard_map/all_to_all | solution.py:168
  97.2 13.5 %all_gather.3 = bf16[128,2048]{1,0:T(8,128)(2,1)S(1)} all-gather(bf16[128,256]{1,0:T(8,128)(2,1)S(1)} %copy-done.12), channel_id=1, replica_groups=mesh['kv'=64,'tp'=8] {'tp'}, dimensions={1}, use_global_device_ids=true | all-gather | bytes 589824 | tf_op jit(solution)/shard_map/all_gather | solution.py:187
  110.6 0.3 fusion.6
  111.1 0.3 fusion
  111.4 1.0 copy.101
  112.4 2.6 %all-to-all-done.2 = bf16[64,2,1,2048]{3,1,2,0:T(2,128)(2,1)S(1)} async-done(((bf16[64,2,1,2048]{3,1,2,0:T(2,128)(2,1)}), bf16[64,2,1,2048]{3,1,2,0:T(2,128)(2,1)S(1)}, u32[]{:S(2)}, u32[]{:S(2)}) %all-to-all-start.2) | async-done | bytes 524320 | tf_op jit(solution)/shard_map/all_to_all | solution.py:168
  115.0 10.1 %all-to-all-start.3 = ((bf16[64,32,128]{2,1,0:T(8,128)(2,1)}), bf16[64,32,128]{2,1,0:T(8,128)(2,1)S(1)}, u32[]{:S(2)}, u32[]{:S(2)}) async-start(bf16[64,32,128]{2,1,0:T(8,128)(2,1)} %bitcast.30), calls=%async_computation.3 | async-start | bytes 1048576 | tf_op jit(solution)/shard_map/all_to_all | solution.py:36
  125.2 1.2 reshape.230
  126.4 0.3 copy.93
  126.7 0.5 fusion.31
  127.6 0.7 convert_element_type.87
  128.5 0.3 copy.98
  128.7 0.5 fusion.29
  129.4 1.0 fusion.19
  130.5 0.7 convert_element_type.93
  131.3 13.6 %all-to-all-done.3 = bf16[64,32,128]{2,1,0:T(8,128)(2,1)S(1)} async-done(((bf16[64,32,128]{2,1,0:T(8,128)(2,1)}), bf16[64,32,128]{2,1,0:T(8,128)(2,1)S(1)}, u32[]{:S(2)}, u32[]{:S(2)}) %all-to-all-start.3) | async-done | bytes 524320 | tf_op jit(solution)/shard_map/all_to_all | solution.py:36
  144.9 0.7 convert_reduce_fusion
  (94 shorter events, 5.5 us)
Async XLA Ops:
  0.6 3.0 %copy-start.7 = (bf16[128,128]{1,0:T(8,128)(2,1)S(1)}, bf16[128,128]{1,0:T(8,128)(2,1)}, u32[]{:S(2)}) copy-start(bf16[128,128]{1,0:T(8,128)(2,1)} %param.13) | copy-start | bytes 98308
  8.7 16.9 %copy-start.8 = (bf16[128,128]{1,0:T(8,128)(2,1)S(1)}, bf16[128,128]{1,0:T(8,128)(2,1)}, u32[]{:S(2)}) copy-start(bf16[128,128]{1,0:T(8,128)(2,1)} %param.12) | copy-start | bytes 98308
  8.7 17.1 %copy-start.13 = (s32[2,256,12]{1,0,2:T(2,128)S(1)}, s32[2,256,12]{1,0,2:T(2,128)}, u32[]{:S(2)}) copy-start(s32[2,256,12]{1,0,2:T(2,128)} %param.16) | copy-start | bytes 73732
  8.7 17.4 %copy-start.14 = (bf16[128,128]{1,0:T(8,128)(2,1)S(1)}, bf16[128,128]{1,0:T(8,128)(2,1)}, u32[]{:S(2)}) copy-start(bf16[128,128]{1,0:T(8,128)(2,1)} %param.14) | copy-start | bytes 98308
  8.7 17.5 %copy-start.16 = (f32[2,128]{1,0:T(2,128)S(1)}, f32[2,128]{1,0:T(2,128)}, u32[]{:S(2)}) copy-start(f32[2,128]{1,0:T(2,128)} %param.15) | copy-start | bytes 3076
  8.7 17.7 %copy-start.15 = (bf16[128,128]{1,0:T(8,128)(2,1)S(1)}, bf16[128,128]{1,0:T(8,128)(2,1)}, u32[]{:S(2)}) copy-start(bf16[128,128]{1,0:T(8,128)(2,1)} %param.11) | copy-start | bytes 98308
  8.7 46.0 %all-to-all-start = ((bf16[64,4,1,2048]{3,1,2,0:T(4,128)(2,1)}), bf16[64,4,1,2048]{3,1,2,0:T(4,128)(2,1)S(1)}, u32[]{:S(2)}, u32[]{:S(2)}) async-start(bf16[64,4,1,2048]{3,1,2,0:T(4,128)(2,1)} %pad_maximum_fusion), calls=%async_computation | async-start | bytes 2097152 | tf_op jit(solution)/shard_map/all_to_all | solution.py:18
  26.4 33.8 %copy-start.10 = (bf16[4,32,2,64]{1,3,0,2:T(8,128)(2,1)}, bf16[4,32,2,64]{1,3,0,2:T(8,128)(2,1)S(1)}, u32[]{:S(2)}) copy-start(bf16[4,32,2,64]{1,3,0,2:T(8,128)(2,1)S(1)} %copy.83) | copy-start | bytes 98308
  59.9 0.8 copy-start.5
  60.7 0.8 copy-start.1
  60.8 0.8 copy-start.3
  64.7 8.4 %copy-start.2 = (f32[2,4,32,416]{3,2,1,0:T(8,128)S(1)}, f32[2,4,32,416]{3,2,1,0:T(8,128)}, u32[]{:S(2)}) copy-start(f32[2,4,32,416]{3,2,1,0:T(8,128)} %copy-done.1) | copy-start | bytes 1277956
  65.9 25.6 %all-to-all-start.1 = ((bf16[64,2,1,2048]{3,1,2,0:T(2,128)(2,1)}), bf16[64,2,1,2048]{3,1,2,0:T(2,128)(2,1)}, u32[]{:S(2)}, u32[]{:S(2)}) async-start(bf16[64,2,1,2048]{3,1,2,0:T(2,128)(2,1)} %bitcast.18), calls=%async_computation.1 | async-start | bytes 1048576 | tf_op jit(solution)/shard_map/all_to_all | solution.py:165
  73.4 1.0 copy-start
  77.4 19.7 %copy-start.12 = (bf16[128,256]{1,0:T(8,128)(2,1)S(1)}, bf16[128,256]{1,0:T(8,128)(2,1)}, u32[]{:S(2)}) copy-start(bf16[128,256]{1,0:T(8,128)(2,1)} %param.17) | copy-start | bytes 196612
  77.5 33.1 %copy-start.4 = (bf16[2,4,32,416]{3,2,1,0:T(8,128)(2,1)S(1)}, bf16[2,4,32,416]{3,2,1,0:T(8,128)(2,1)}, u32[]{:S(2)}) copy-start(bf16[2,4,32,416]{3,2,1,0:T(8,128)(2,1)} %copy-done.3) | copy-start | bytes 638980
  77.5 33.1 %copy-start.6 = (bf16[2,4,384,64]{2,3,1,0:T(8,128)(2,1)S(1)}, bf16[2,4,384,64]{2,3,1,0:T(8,128)(2,1)}, u32[]{:S(2)}) copy-start(bf16[2,4,384,64]{2,3,1,0:T(8,128)(2,1)} %copy-done.5) | copy-start | bytes 1179652
  77.5 33.1 %copy-start.11 = (bf16[4,32,2,64]{1,3,0,2:T(8,128)(2,1)S(1)}, bf16[4,32,2,64]{1,3,0,2:T(8,128)(2,1)}, u32[]{:S(2)}) copy-start(bf16[4,32,2,64]{1,3,0,2:T(8,128)(2,1)} %copy-done.10) | copy-start | bytes 98308
  91.5 23.6 %all-to-all-start.2 = ((bf16[64,2,1,2048]{3,1,2,0:T(2,128)(2,1)}), bf16[64,2,1,2048]{3,1,2,0:T(2,128)(2,1)S(1)}, u32[]{:S(2)}, u32[]{:S(2)}) async-start(bf16[64,2,1,2048]{3,1,2,0:T(2,128)(2,1)} %bitcast.24), calls=%async_computation.2 | async-start | bytes 1048576 | tf_op jit(solution)/shard_map/all_to_all | solution.py:168
  111.1 3.9 %copy-start.9 = (bf16[128,128]{1,0:T(8,128)(2,1)}, bf16[128,128]{1,0:T(8,128)(2,1)S(1)}, u32[]{:S(2)}) copy-start(bf16[128,128]{1,0:T(8,128)(2,1)S(1)} %convert_element_type.82) | copy-start | bytes 98308
  115.0 29.8 %all-to-all-start.3 = ((bf16[64,32,128]{2,1,0:T(8,128)(2,1)}), bf16[64,32,128]{2,1,0:T(8,128)(2,1)S(1)}, u32[]{:S(2)}, u32[]{:S(2)}) async-start(bf16[64,32,128]{2,1,0:T(8,128)(2,1)} %bitcast.30), calls=%async_computation.3 | async-start | bytes 1048576 | tf_op jit(solution)/shard_map/all_to_all | solution.py:36
where the time goes:
time: 146 us
  waiting for transfers between devices  56.8 us (39%)
  starting transfers between devices  39.4 us (27%)
  local copies, waits for them, and re-layouts  22.7 us (16%)
  blocking collectives  13.5 us (9%)
  other arithmetic  8.99 us (6%)
  matrix products  2.89 us (2%)
    all_to_all x1, waiting for transfers between devices, sent_together(): lax.all_to_all(both, axis, split_axis=split_dim, concat_axis=concat_dim,...  27.8 us
    all_to_all x1, starting transfers between devices, sent_together(): lax.all_to_all(both, axis, split_axis=split_dim, concat_axis=concat_dim,...  16.7 us
    all_to_all x1, waiting for transfers between devices, sum_at_owner(): lax.all_to_all(tiles, axis, split_axis=0, concat_axis=0, tiled=True)  13.6 us
    all_gather x1, blocking collectives, body(): whole_input = lax.all_gather(normed_input, 'tp', axis=1, tiled=True)  13.5 us
    all_to_all x1, waiting for transfers between devices, body(): lax.all_to_all(to_slots(key_grad).astype(jnp.bfloat16), 'kv', split_axis=...  12.8 us
    all_to_all x1, starting transfers between devices, sum_at_owner(): lax.all_to_all(tiles, axis, split_axis=0, concat_axis=0, tiled=True)  10.1 us
    all_to_all x1, starting transfers between devices, body(): lax.all_to_all(to_slots(key_grad).astype(jnp.bfloat16), 'kv', split_axis=...  7.14 us
    all_to_all x1, starting transfers between devices, body(): lax.all_to_all(to_slots(value_grad).astype(jnp.bfloat16), 'kv', split_axi...  5.45 us
  transfers between devices with their start and end apart: 4, of which 4 were waited for; matrix products, arithmetic and copies ran while one was open for 10% of the time, Pallas kernels for 0%

commit v1 on v0

v1 whole, which is shorter than its diff:
```python
import jax
import jax.numpy as jnp
from jax import lax
from jax.experimental import pallas as pl
from jax.experimental.pallas import tpu as pltpu
from jax.sharding import PartitionSpec as P

HD = 64
BLK = 32
SEL = 12
MASKED = -1e30

F32 = jnp.float32
BF16 = jnp.bfloat16
VMEM = pl.BlockSpec(memory_space=pltpu.VMEM)
SMEM = pl.BlockSpec(memory_space=pltpu.SMEM)
NT = (((1,), (1,)), ((), ()))
NN = (((1,), (0,)), ((), ()))
TN = (((0,), (0,)), ((), ()))


def dot(a, b, dims):
    return lax.dot_general(a, b, dims, preferred_element_type=F32)


def pick_kernel(me_ref, chosen_ref, k_ref, v_ref, send_ref, ids_ref):
    heads, blocks, sel = chosen_ref.shape
    devices = send_ref.shape[0]
    blocks_dev = blocks // devices
    width = k_ref.shape[1]
    first = me_ref[0] * blocks_dev
    row = lax.broadcasted_iota(jnp.int32, (blocks, sel), 0)
    lane = lax.broadcasted_iota(jnp.int32, (blocks, width), 1)
    codes = jnp.zeros((blocks, width), F32)
    for h in range(heads):
        c = chosen_ref[h]
        d = c - first
        hit = (c < row) & (d >= 0) & (d < blocks_dev)
        code = jnp.where(hit, jnp.left_shift(1, 3 * jnp.where(hit, d, 0)), 0).astype(F32)
        codes = jnp.where(lane // HD == h, jnp.sum(code, axis=1, keepdims=True), codes)
    owner = lax.broadcasted_iota(jnp.int32, (devices, blocks), 0)
    block = lax.broadcasted_iota(jnp.int32, (devices, blocks), 1)
    group = jnp.where(block // blocks_dev == owner, 1.0, 0.0).astype(BF16)
    ids_ref[...] = dot(group, codes.astype(BF16), NN)
    kb = [k_ref[b * BLK : (b + 1) * BLK, :].astype(F32) for b in range(blocks_dev)]
    vb = [v_ref[b * BLK : (b + 1) * BLK, :].astype(F32) for b in range(blocks_dev)]

    def step(t, _):
        code = jnp.broadcast_to(ids_ref[pl.ds(t, 1), :], (BLK, width))
        ks, vs = kb[0], vb[0]
        for b in range(1, blocks_dev):
            m = code >= 8.0**b
            ks = jnp.where(m, kb[b], ks)
            vs = jnp.where(m, vb[b], vs)
        send_ref[t, 0:BLK, :] = ks.astype(BF16)
        send_ref[t, BLK : 2 * BLK, :] = vs.astype(BF16)
        return 0

    lax.fori_loop(0, devices, step, 0, unroll=4)


def grad_kernel(
    tiles_ref, q_ref, g_ref, k_ref, v_ref, bias_ref, lse_ref, xt_ref,
    send_ref, dq_ref, dk_ref, dv_ref, p_ref, d_ref,
):
    devices = tiles_ref.shape[0]
    rows, width = q_ref.shape
    heads = width // HD
    cols = heads * rows
    scale = HD**-0.5
    step_slots = 8
    chunk = step_slots * BLK
    lane = lax.broadcasted_iota(jnp.int32, (rows, width), 1)

    def by_head(x):
        return jnp.concatenate(
            [jnp.where(lane // HD == h, x, 0.0).astype(BF16) for h in range(heads)], axis=0
        )

    qm = by_head(q_ref[...].astype(F32))
    gm = by_head(g_ref[...].astype(F32))

    ko, vo = k_ref[...], v_ref[...]
    key_row = lax.broadcasted_iota(jnp.int32, (rows, cols), 0)
    query = lax.broadcasted_iota(jnp.int32, (rows, cols), 1) % rows
    own = (key_row // BLK == query // BLK) & (key_row <= query)
    p_own = jnp.exp(jnp.where(own, dot(ko, qm, NT) * scale - lse_ref[...], MASKED))
    d_own = dot(vo, gm, NT)
    delta0 = jnp.sum((p_own * d_own).reshape(rows // 8, 8, cols), axis=0)

    def forward(c, delta):
        keys = tiles_ref[pl.ds(c * step_slots, step_slots), 0:BLK, :].reshape(chunk, width)
        vals = tiles_ref[pl.ds(c * step_slots, step_slots), BLK : 2 * BLK, :].reshape(chunk, width)
        s = dot(keys, qm, NT) * scale
        d = dot(vals, gm, NT)
        for i in range(step_slots):
            b = bias_ref[pl.ds(c * step_slots + i, 1), :]
            sl = slice(i * BLK, (i + 1) * BLK)
            p = jnp.exp(s[sl] + b)
            at = pl.ds(pl.multiple_of(c * chunk + i * BLK, BLK), BLK)
            p_ref[at, :] = p
            d_ref[at, :] = d[sl]
            delta = delta + jnp.sum((p * d[sl]).reshape(BLK // 8, 8, cols), axis=0)
        return delta

    steps = devices // step_slots
    delta = lax.fori_loop(0, steps, forward, delta0, unroll=2)
    delta = jnp.sum(delta, axis=0, keepdims=True)

    ds_own = (p_own * (d_own - delta)).astype(BF16)
    dk_ref[...] = dot(ds_own, qm, NN) * scale
    dv_ref[...] = dot(p_own.astype(BF16), gm, NN)
    dqt0 = dot(ko, ds_own, TN)

    def backward(c, dqt):
        at = pl.ds(pl.multiple_of(c * chunk, chunk), chunk)
        p = p_ref[at, :]
        ds = (p * (d_ref[at, :] - delta)).astype(BF16)
        keys = tiles_ref[pl.ds(c * step_slots, step_slots), 0:BLK, :].reshape(chunk, width)
        dk = (dot(ds, qm, NN) * scale).astype(BF16)
        dv = dot(p.astype(BF16), gm, NN).astype(BF16)
        slots = pl.ds(c * step_slots, step_slots)
        send_ref[slots, 0:BLK, :] = dk.reshape(step_slots, BLK, width)
        send_ref[slots, BLK : 2 * BLK, :] = dv.reshape(step_slots, BLK, width)
        return dqt + dot(keys, ds, TN)

    dqt = lax.fori_loop(0, steps, backward, dqt0, unroll=2)
    head_of = lax.broadcasted_iota(jnp.int32, (width, rows), 0) // HD
    merged = dqt[:, 0:rows]
    for h in range(1, heads):
        merged = jnp.where(head_of == h, dqt[:, h * rows : (h + 1) * rows], merged)
    dq = (jnp.transpose(merged) * scale).astype(BF16)
    dq_ref[...] = dq
    piece = xt_ref.shape[0] // devices
    w = dot(xt_ref[...], dq, NN).astype(BF16)
    send_ref[:, 2 * BLK : 2 * BLK + piece, :] = w.reshape(devices, piece, width)


def settle_kernel(back_ref, ids_ref, dk_ref, dv_ref, gk_ref, gv_ref, gw_ref):
    devices = back_ref.shape[0]
    rows, width = dk_ref.shape
    blocks_dev = rows // BLK
    piece = gw_ref.shape[0]
    start = tuple(dk_ref[b * BLK : (b + 1) * BLK, :] for b in range(blocks_dev))
    start += tuple(dv_ref[b * BLK : (b + 1) * BLK, :] for b in range(blocks_dev))
    start += (jnp.zeros((piece, width), F32),)

    def step(t, sums):
        code = jnp.broadcast_to(ids_ref[pl.ds(t, 1), :], (BLK, width))
        dk = back_ref[t, 0:BLK, :].astype(F32)
        dv = back_ref[t, BLK : 2 * BLK, :].astype(F32)
        w = back_ref[t, 2 * BLK : 2 * BLK + piece, :].astype(F32)
        out_k, out_v = [], []
        for b in range(blocks_dev):
            m = (code >= 8.0**b) & (code < 8.0 ** (b + 1))
            out_k.append(sums[b] + jnp.where(m, dk, 0.0))
            out_v.append(sums[blocks_dev + b] + jnp.where(m, dv, 0.0))
        return tuple(out_k) + tuple(out_v) + (sums[-1] + w,)

    sums = lax.fori_loop(0, devices, step, start, unroll=2)
    for b in range(blocks_dev):
        gk_ref[b * BLK : (b + 1) * BLK, :] = sums[b].astype(BF16)
        gv_ref[b * BLK : (b + 1) * BLK, :] = sums[blocks_dev + b].astype(BF16)
    gw_ref[...] = sums[-1]


def body(queries, keys, values, cotangent, log_sum, chosen, normed_input):
    rows, width = queries.shape
    heads, block_total, _ = chosen.shape
    blocks_dev = rows // BLK
    devices = lax.axis_size("kv")
    me = lax.axis_index("kv")
    shape = jax.ShapeDtypeStruct

    send, ids = pl.pallas_call(
        pick_kernel,
        out_shape=(shape((devices, 2 * BLK, width), BF16), shape((devices, width), F32)),
        in_specs=[SMEM, VMEM, VMEM, VMEM],
        out_specs=(VMEM, VMEM),
        name="pick",
    )(me.astype(jnp.int32).reshape(1), chosen, keys, values)
    tiles = lax.all_to_all(send, "kv", split_axis=0, concat_axis=0, tiled=True)

    xt = lax.all_gather(normed_input.T, "tp", axis=0, tiled=True)
    own_ids = me * blocks_dev + jnp.arange(blocks_dev, dtype=jnp.int32)
    lists = lax.dynamic_slice_in_dim(chosen, me * blocks_dev, blocks_dev, 1)
    owners = jnp.where(lists < own_ids[None, :, None], lists // blocks_dev, -1)
    slots = jnp.arange(devices, dtype=jnp.int32)
    asked = jnp.any(owners[None] == slots[:, None, None, None], axis=-1)
    bias = jnp.where(
        asked[..., None], -log_sum.reshape(1, heads, blocks_dev, BLK), MASKED
    ).reshape(devices, heads * rows)
    lse = log_sum.reshape(1, heads * rows)

    piece = xt.shape[0] // devices
    send2, dq, dk, dv = pl.pallas_call(
        grad_kernel,
        out_shape=(
            shape((devices, 2 * BLK + piece, width), BF16),
            shape((rows, width), BF16),
            shape((rows, width), F32),
            shape((rows, width), F32),
        ),
        in_specs=[VMEM] * 8,
        out_specs=(VMEM,) * 4,
        scratch_shapes=[
            pltpu.VMEM((devices * BLK, heads * rows), F32),
            pltpu.VMEM((devices * BLK, heads * rows), F32),
        ],
        name="grads",
    )(tiles, queries, cotangent, keys, values, bias, lse, xt)
    back = lax.all_to_all(send2, "kv", split_axis=0, concat_axis=0, tiled=True)
    gk, gv, gw = pl.pallas_call(
        settle_kernel,
        out_shape=(
            shape((rows, width), BF16),
            shape((rows, width), BF16),
            shape((piece, width), F32),
        ),
        in_specs=[VMEM] * 4,
        out_specs=(VMEM,) * 3,
        name="settle",
    )(back, ids, dk, dv)
    return (dq, gk, gv, gw)


def solution(mesh):
    in_specs = (
        P("kv", "tp"),
        P("kv", "tp"),
        P("kv", "tp"),
        P("kv", "tp"),
        P("tp", "kv"),
        P("tp", None, None),
        P("kv", "tp"),
    )
    out_specs = (P("kv", "tp"), P("kv", "tp"), P("kv", "tp"), P("kv", "tp"))
    return jax.shard_map(body, mesh=mesh, in_specs=in_specs, out_specs=out_specs, check_vma=False)
```

time: 146 us -> 109 us (0.75)
  the two profiles are of different devices: /device:TPU:8 before, /device:TPU:4 now
where the time goes in v1:
time: 109 us
  blocking collectives  60.1 us (55%)
  starting transfers between devices  16.6 us (15%)
  waiting for transfers between devices  15.6 us (14%)
  Pallas kernels  11.9 us (11%)
  local copies, waits for them, and re-layouts  2.85 us (3%)
    all_to_all x1, blocking collectives, body(): back = lax.all_to_all(send2, 'kv', split_axis=0, concat_axis=0, tiled=True)  47.2 us
    all_to_all x1, starting transfers between devices, body(): tiles = lax.all_to_all(send, 'kv', split_axis=0, concat_axis=0, tiled=True)  16.6 us
    all_to_all x1, waiting for transfers between devices, body(): tiles = lax.all_to_all(send, 'kv', split_axis=0, concat_axis=0, tiled=True)  15.6 us
    all_gather x1, blocking collectives, body(): xt = lax.all_gather(normed_input.T, 'tp', axis=0, tiled=True)  13 us
    pallas_call x1, Pallas kernels, body(): pl.pallas_call(grad_kernel, out_shape=(shape((devices, 2 * BLK + piece, w...  5.99 us
    pallas_call x1, Pallas kernels, body(): pl.pallas_call(settle_kernel, out_shape=(shape((rows, width), BF16), shap...  3.25 us
    unnamed x10, local copies, waits for them, and re-layouts  2.73 us
    pallas_call x1, Pallas kernels, body(): pl.pallas_call(pick_kernel, out_shape=(shape((devices, 2 * BLK, width), B...  2.62 us
  transfers between devices with their start and end apart: 1, of which 1 were waited for; matrix products, arithmetic and copies ran while one was open for 1% of the time, Pallas kernels for 0%

profile of v1, /device:TPU:4, one launch (start us, length us, event | category | flops | bytes accessed | tf_op | source)
XLA Modules:
  0.0 108.7 jit_solution(18326562621838714050)
XLA Ops:
  0.6 0.0 copy-start.2
  0.6 0.0 copy-start.1
  0.7 0.0 copy-start.3
  0.7 1.6 %copy.18.chosen_ref = s32[2,256,12]{2,1,0:T(8,128)} copy(s32[2,256,12]{1,0,2:T(2,128)} %param.12) | data formatting | bytes 49152 | tf_op args[5]
  2.3 2.6 %pick.1 = (bf16[64,64,128]{2,1,0:T(8,128)(2,1)}, f32[64,128]{1,0:T(8,128)}) custom-call(s32[1]{0:T(128)} %bitcast.me_ref, s32[2,256,12]{2,1,0:T(8,128)} %copy.18.chosen_ref, bf16[128,128]{1,0:T(8,128)(2,1)} %k_ref.3, bf16[128,128]{1,0:T(8,128)(2,1)} %v_ref.3), custom_call_target="tpu_custom_call" | custom-call | tf_op jit(solution)/shard_map/pick/pallas_call | solution.py:175
  4.9 16.6 %all-to-all-start = ((bf16[64,64,128]{2,1,0:T(8,128)(2,1)}), bf16[64,64,128]{2,1,0:T(8,128)(2,1)S(1)}, u32[]{:S(2)}, u32[]{:S(2)}) async-start(bf16[64,64,128]{2,1,0:T(8,128)(2,1)} %get-tuple-element.13), calls=%async_computation | async-start | bytes 2097152 | tf_op jit(solution)/shard_map/all_to_all | solution.py:182
  21.5 0.0 copy-done.2
  21.5 0.1 compare_select_fusion
  21.7 0.1 fusion
  21.8 0.1 copy.20
  21.9 0.0 copy-done.1
  21.9 0.1 copy.21
  22.0 0.0 copy-done.3
  22.0 0.6 broadcast_select_fusion.bias_ref
  22.7 13.0 %all_gather.3.xt_ref = bf16[2048,128]{1,0:T(8,128)(2,1)} all-gather(bf16[256,128]{1,0:T(8,128)(2,1)S(1)} %bitcast.6), channel_id=1, replica_groups=mesh['kv'=64,'tp'=8] {'tp'}, dimensions={0}, use_global_device_ids=true | all-gather | bytes 589824 | tf_op jit(solution)/shard_map/all_gather | solution.py:184
  35.6 15.6 %all-to-all-done.tiles_ref = bf16[64,64,128]{2,1,0:T(8,128)(2,1)S(1)} async-done(((bf16[64,64,128]{2,1,0:T(8,128)(2,1)}), bf16[64,64,128]{2,1,0:T(8,128)(2,1)S(1)}, u32[]{:S(2)}, u32[]{:S(2)}) %all-to-all-start) | async-done | bytes 1048608 | tf_op jit(solution)/shard_map/all_to_all | solution.py:182
  51.3 0.0 copy-start
  51.3 1.0 copy-done
  52.3 6.0 %grads.1 = (bf16[64,96,128]{2,1,0:T(8,128)(2,1)}, bf16[128,128]{1,0:T(8,128)(2,1)}, f32[128,128]{1,0:T(8,128)}, f32[128,128]{1,0:T(8,128)}) custom-call(bf16[64,64,128]{2,1,0:T(8,128)(2,1)} %copy-done, bf16[128,128]{1,0:T(8,128)(2,1)} %q_ref.1, bf16[128,128]{1,0:T(8,128)(2,1)} %g_ref.1, bf16[128,128]{1,0:T(8,128)(2,1)} %k_ref.3, bf16[128,128]{1,0:T(8,128)(2,1)} %v_ref.3, ...), custom_call_target="tpu_custom_call" | custom-call | tf_op jit(solution)/shard_map/grads/pallas_call | solution.py:196
  58.2 47.2 %all_to_all.10.back_ref = bf16[64,96,128]{2,1,0:T(8,128)(2,1)} all-to-all(bf16[64,96,128]{2,1,0:T(8,128)(2,1)} %get-tuple-element.15), channel_id=1, replica_groups=mesh['kv'=64,'tp'=8] {'kv'}, dimensions={0} | all-to-all | bytes 3145728 | tf_op jit(solution)/shard_map/all_to_all | solution.py:212
  105.4 3.3 %settle.1 = (bf16[128,128]{1,0:T(8,128)(2,1)}, bf16[128,128]{1,0:T(8,128)(2,1)}, f32[32,128]{1,0:T(8,128)}) custom-call(bf16[64,96,128]{2,1,0:T(8,128)(2,1)} %all_to_all.10.back_ref, f32[64,128]{1,0:T(8,128)} %get-tuple-element.16.ids_ref, f32[128,128]{1,0:T(8,128)} %get-tuple-element.17.dk_ref, f32[128,128]{1,0:T(8,128)} %get-tuple-element.18.dv_ref), custom_call_target="tpu_custom_call" | custom-call | tf_op jit(solution)/shard_map/settle/pallas_call | solution.py:213
  (4 shorter events, 0.0 us)
Async XLA Ops:
  0.6 20.9 %copy-start.2 = (s32[2,256,12]{1,0,2:T(2,128)S(1)}, s32[2,256,12]{1,0,2:T(2,128)}, u32[]{:S(2)}) copy-start(s32[2,256,12]{1,0,2:T(2,128)} %param.12) | copy-start | bytes 73732
  0.6 21.3 %copy-start.1 = (bf16[128,256]{1,0:T(8,128)(2,1)S(1)}, bf16[128,256]{1,0:T(8,128)(2,1)}, u32[]{:S(2)}) copy-start(bf16[128,256]{1,0:T(8,128)(2,1)} %param.13) | copy-start | bytes 196612
  0.7 21.4 %copy-start.3 = (f32[2,128]{1,0:T(2,128)S(1)}, f32[2,128]{1,0:T(2,128)}, u32[]{:S(2)}) copy-start(f32[2,128]{1,0:T(2,128)} %param.11) | copy-start | bytes 3076
  4.9 46.4 %all-to-all-start = ((bf16[64,64,128]{2,1,0:T(8,128)(2,1)}), bf16[64,64,128]{2,1,0:T(8,128)(2,1)S(1)}, u32[]{:S(2)}, u32[]{:S(2)}) async-start(bf16[64,64,128]{2,1,0:T(8,128)(2,1)} %get-tuple-element.13), calls=%async_computation | async-start | bytes 2097152 | tf_op jit(solution)/shard_map/all_to_all | solution.py:182
  51.3 1.0 copy-start

commit v2 on v1

--- a/solution.py
+++ b/solution.py
@@ -24,24 +24,26 @@
 
 
 def pick_kernel(me_ref, chosen_ref, k_ref, v_ref, send_ref, ids_ref):
-    heads, blocks, sel = chosen_ref.shape
+    sel, heads, blocks = chosen_ref.shape
     devices = send_ref.shape[0]
     blocks_dev = blocks // devices
     width = k_ref.shape[1]
     first = me_ref[0] * blocks_dev
-    row = lax.broadcasted_iota(jnp.int32, (blocks, sel), 0)
-    lane = lax.broadcasted_iota(jnp.int32, (blocks, width), 1)
-    codes = jnp.zeros((blocks, width), F32)
-    for h in range(heads):
-        c = chosen_ref[h]
-        d = c - first
-        hit = (c < row) & (d >= 0) & (d < blocks_dev)
-        code = jnp.where(hit, jnp.left_shift(1, 3 * jnp.where(hit, d, 0)), 0).astype(F32)
-        codes = jnp.where(lane // HD == h, jnp.sum(code, axis=1, keepdims=True), codes)
+    d = chosen_ref[...] - first
+    asking = lax.broadcasted_iota(jnp.int32, (sel, heads, blocks), 2) - first
+    hit = (d < asking) & (d >= 0) & (d < blocks_dev)
+    code = jnp.zeros(d.shape, F32)
+    for b in range(blocks_dev):
+        code = jnp.where(hit & (d == b), 8.0**b, code)
+    code = jnp.sum(code, axis=0)
+    row = lax.broadcasted_iota(jnp.int32, (width, blocks), 0)
+    codes = jnp.broadcast_to(code[0:1, :], (width, blocks))
+    for h in range(1, heads):
+        codes = jnp.where(row // HD == h, code[h : h + 1, :], codes)
     owner = lax.broadcasted_iota(jnp.int32, (devices, blocks), 0)
     block = lax.broadcasted_iota(jnp.int32, (devices, blocks), 1)
     group = jnp.where(block // blocks_dev == owner, 1.0, 0.0).astype(BF16)
-    ids_ref[...] = dot(group, codes.astype(BF16), NN)
+    ids_ref[...] = dot(group, codes.astype(BF16), NT)
     kb = [k_ref[b * BLK : (b + 1) * BLK, :].astype(F32) for b in range(blocks_dev)]
     vb = [v_ref[b * BLK : (b + 1) * BLK, :].astype(F32) for b in range(blocks_dev)]
 
@@ -80,18 +82,18 @@
     qm = by_head(q_ref[...].astype(F32))
     gm = by_head(g_ref[...].astype(F32))
 
-    ko, vo = k_ref[...], v_ref[...]
+    ko, vo = (k_ref[...].astype(F32) * scale).astype(BF16), v_ref[...]
     key_row = lax.broadcasted_iota(jnp.int32, (rows, cols), 0)
     query = lax.broadcasted_iota(jnp.int32, (rows, cols), 1) % rows
     own = (key_row // BLK == query // BLK) & (key_row <= query)
-    p_own = jnp.exp(jnp.where(own, dot(ko, qm, NT) * scale - lse_ref[...], MASKED))
+    p_own = jnp.exp(jnp.where(own, dot(ko, qm, NT) - lse_ref[...], MASKED))
     d_own = dot(vo, gm, NT)
     delta0 = jnp.sum((p_own * d_own).reshape(rows // 8, 8, cols), axis=0)
 
     def forward(c, delta):
         keys = tiles_ref[pl.ds(c * step_slots, step_slots), 0:BLK, :].reshape(chunk, width)
         vals = tiles_ref[pl.ds(c * step_slots, step_slots), BLK : 2 * BLK, :].reshape(chunk, width)
-        s = dot(keys, qm, NT) * scale
+        s = dot(keys, qm, NT)
         d = dot(vals, gm, NT)
         for i in range(step_slots):
             b = bias_ref[pl.ds(c * step_slots + i, 1), :]
@@ -129,7 +131,7 @@
     merged = dqt[:, 0:rows]
     for h in range(1, heads):
         merged = jnp.where(head_of == h, dqt[:, h * rows : (h + 1) * rows], merged)
-    dq = (jnp.transpose(merged) * scale).astype(BF16)
+    dq = jnp.transpose(merged).astype(BF16)
     dq_ref[...] = dq
     piece = xt_ref.shape[0] // devices
     w = dot(xt_ref[...], dq, NN).astype(BF16)
@@ -146,15 +148,15 @@
     start += (jnp.zeros((piece, width), F32),)
 
     def step(t, sums):
-        code = jnp.broadcast_to(ids_ref[pl.ds(t, 1), :], (BLK, width))
+        code = ids_ref[pl.ds(t, 1), :]
         dk = back_ref[t, 0:BLK, :].astype(F32)
         dv = back_ref[t, BLK : 2 * BLK, :].astype(F32)
         w = back_ref[t, 2 * BLK : 2 * BLK + piece, :].astype(F32)
         out_k, out_v = [], []
         for b in range(blocks_dev):
-            m = (code >= 8.0**b) & (code < 8.0 ** (b + 1))
-            out_k.append(sums[b] + jnp.where(m, dk, 0.0))
-            out_v.append(sums[blocks_dev + b] + jnp.where(m, dv, 0.0))
+            m = jnp.where((code >= 8.0**b) & (code < 8.0 ** (b + 1)), 1.0, 0.0)
+            out_k.append(sums[b] + m * dk)
+            out_v.append(sums[blocks_dev + b] + m * dv)
         return tuple(out_k) + tuple(out_v) + (sums[-1] + w,)
 
     sums = lax.fori_loop(0, devices, step, start, unroll=2)
@@ -172,14 +174,20 @@
     me = lax.axis_index("kv")
     shape = jax.ShapeDtypeStruct
 
+    def near(x):
+        return pltpu.with_memory_space_constraint(x, pltpu.VMEM)
+
     send, ids = pl.pallas_call(
         pick_kernel,
-        out_shape=(shape((devices, 2 * BLK, width), BF16), shape((devices, width), F32)),
+        out_shape=(pltpu.VMEM((devices, 2 * BLK, width), BF16), pltpu.VMEM((devices, width), F32)),
         in_specs=[SMEM, VMEM, VMEM, VMEM],
         out_specs=(VMEM, VMEM),
         name="pick",
-    )(me.astype(jnp.int32).reshape(1), chosen, keys, values)
+    )(me.astype(jnp.int32).reshape(1), near(chosen.transpose(2, 0, 1)), near(keys), near(values))
     tiles = lax.all_to_all(send, "kv", split_axis=0, concat_axis=0, tiled=True)
+
+    key_rows = jnp.arange(2 * BLK) < BLK
+    tiles = tiles * jnp.where(key_rows, HD**-0.5, 1.0).astype(BF16)[None, :, None]
 
     xt = lax.all_gather(normed_input.T, "tp", axis=0, tiled=True)
     own_ids = me * blocks_dev + jnp.arange(blocks_dev, dtype=jnp.int32)
@@ -196,10 +204,10 @@
     send2, dq, dk, dv = pl.pallas_call(
         grad_kernel,
         out_shape=(
-            shape((devices, 2 * BLK + piece, width), BF16),
+            pltpu.VMEM((devices, 2 * BLK + piece, width), BF16),
             shape((rows, width), BF16),
-            shape((rows, width), F32),
-            shape((rows, width), F32),
+            pltpu.VMEM((rows, width), F32),
+            pltpu.VMEM((rows, width), F32),
         ),
         in_specs=[VMEM] * 8,
         out_specs=(VMEM,) * 4,
@@ -208,7 +216,7 @@
             pltpu.VMEM((devices * BLK, heads * rows), F32),
         ],
         name="grads",
-    )(tiles, queries, cotangent, keys, values, bias, lse, xt)
+    )(*map(near, (tiles, queries, cotangent, keys, values, bias, lse, xt)))
     back = lax.all_to_all(send2, "kv", split_axis=0, concat_axis=0, tiled=True)
     gk, gv, gw = pl.pallas_call(
         settle_kernel,
@@ -220,7 +228,7 @@
         in_specs=[VMEM] * 4,
         out_specs=(VMEM,) * 3,
         name="settle",
-    )(back, ids, dk, dv)
+    )(*map(near, (back, ids, dk, dv)))
     return (dq, gk, gv, gw)
 
 

time: 109 us -> 104 us (0.954)
  Pallas kernels: 11.9 us -> 6.99 us
  waiting for transfers between devices: 15.6 us -> 17.3 us
  blocking collectives: 60.1 us -> 58.7 us
    pallas_call x2, Pallas kernels: 8.61 us -> 5.22 us  [the longest x1 3.69 us: body(): pl.pallas_call(grad_kernel, out_shape=(pltpu.VMEM((devices, 2 * BLK + pie...]
    all_to_all x1, waiting for transfers between devices: 15.6 us -> 17.3 us  [body(): tiles = lax.all_to_all(send, 'kv', split_axis=0, concat_axis=0, tiled=True)]
    pallas_call x1, Pallas kernels: 3.25 us -> 1.77 us  [body(): pl.pallas_call(settle_kernel, out_shape=(shape((rows, width), BF16), shap...]
    unnamed x10 -> x21, local copies, waits for them, and re-layouts: 2.73 us -> 2.4 us
  transfers between devices with their start and end apart: 1 -> 1, of which waited for: 1 -> 1; matrix products, arithmetic and copies ran while one was open for 1% -> 0% of each run, Pallas kernels for 0% -> 0%
where the time goes in v2:
time: 104 us; the launch traced here: 103 us
  blocking collectives  58.7 us (56%)
  waiting for transfers between devices  17.3 us (17%)
  starting transfers between devices  16.6 us (16%)
  Pallas kernels  6.99 us (7%)
  local copies, waits for them, and re-layouts  2.51 us (2%)
    all_to_all x1, blocking collectives, body(): back = lax.all_to_all(send2, 'kv', split_axis=0, concat_axis=0, tiled=True)  46.8 us
    all_to_all x1, waiting for transfers between devices, body(): tiles = lax.all_to_all(send, 'kv', split_axis=0, concat_axis=0, tiled=True)  17.3 us
    all_to_all x1, starting transfers between devices, body(): tiles = lax.all_to_all(send, 'kv', split_axis=0, concat_axis=0, tiled=True)  16.6 us
    all_gather x1, blocking collectives, body(): xt = lax.all_gather(normed_input.T, 'tp', axis=0, tiled=True)  11.9 us
    pallas_call x1, Pallas kernels, body(): pl.pallas_call(grad_kernel, out_shape=(pltpu.VMEM((devices, 2 * BLK + pie...  3.69 us
    unnamed x21, local copies, waits for them, and re-layouts  2.4 us
  transfers between devices with their start and end apart: 1, of which 1 were waited for; matrix products, arithmetic and copies ran while one was open for 0% of the time, Pallas kernels for 0%

profile of v2, /device:TPU:4, one launch (start us, length us, event | category | flops | bytes accessed | tf_op | source)
XLA Modules:
  0.0 103.3 jit_solution(377096416643472462)
XLA Ops:
  0.6 0.0 copy-start.8
  0.6 0.0 copy-start
  0.7 0.7 copy-done
  1.4 0.0 copy-start.2
  1.4 0.8 copy-done.2
  2.2 0.0 copy-start.4
  2.2 0.7 copy-done.4
  2.9 0.0 copy-start.5
  2.9 0.0 copy-start.9
  2.9 1.5 %pick.1 = (bf16[64,64,128]{2,1,0:T(8,128)(2,1)}, f32[64,128]{1,0:T(8,128)S(1)}) custom-call(s32[1]{0:T(128)} %bitcast.me_ref, s32[12,2,256]{2,1,0:T(2,128)S(1)} %bitcast.7, bf16[128,128]{1,0:T(8,128)(2,1)S(1)} %copy-done, bf16[128,128]{1,0:T(8,128)(2,1)S(1)} %copy-done.2), custom_call_target="tpu_custom_call" | custom-call | tf_op jit(solution)/shard_map/pick/pallas_call | solution.py:180
  4.4 16.6 %all-to-all-start = ((bf16[64,64,128]{2,1,0:T(8,128)(2,1)}), bf16[64,64,128]{2,1,0:T(8,128)(2,1)S(1)}, u32[]{:S(2)}, u32[]{:S(2)}) async-start(bf16[64,64,128]{2,1,0:T(8,128)(2,1)} %get-tuple-element.13), calls=%async_computation | async-start | bytes 2097152 | tf_op jit(solution)/shard_map/all_to_all | solution.py:187
  21.0 0.0 copy-start.1
  21.0 0.0 copy-start.3
  21.1 0.0 copy-start.6
  21.1 0.0 copy-start.7
  21.1 0.0 copy-done.5
  21.1 0.1 compare_select_fusion
  21.2 0.1 fusion
  21.4 0.1 copy.17
  21.5 0.0 copy-done.9
  21.5 0.1 copy.18
  21.6 0.0 copy-done.8
  21.6 11.9 %all_gather.3.xt_ref = bf16[2048,128]{1,0:T(8,128)(2,1)S(1)} all-gather(bf16[256,128]{1,0:T(8,128)(2,1)S(1)} %bitcast.9), channel_id=1, replica_groups=mesh['kv'=64,'tp'=8] {'tp'}, dimensions={0}, use_global_device_ids=true | all-gather | bytes 589824 | tf_op jit(solution)/shard_map/all_gather | solution.py:192
  33.5 17.3 %all-to-all-done = bf16[64,64,128]{2,1,0:T(8,128)(2,1)S(1)} async-done(((bf16[64,64,128]{2,1,0:T(8,128)(2,1)}), bf16[64,64,128]{2,1,0:T(8,128)(2,1)S(1)}, u32[]{:S(2)}, u32[]{:S(2)}) %all-to-all-start) | async-done | bytes 1048608 | tf_op jit(solution)/shard_map/all_to_all | solution.py:187
  50.8 0.1 broadcast_multiply_fusion.tiles_ref
  50.9 0.0 copy-done.1
  50.9 0.0 copy-done.3
  50.9 0.0 copy-done.6
  51.0 0.0 copy-done.7
  51.0 3.7 %grads.1 = (bf16[64,96,128]{2,1,0:T(8,128)(2,1)S(1)}, bf16[128,128]{1,0:T(8,128)(2,1)}, f32[128,128]{1,0:T(8,128)S(1)}, f32[128,128]{1,0:T(8,128)S(1)}) custom-call(bf16[64,64,128]{2,1,0:T(8,128)(2,1)S(1)} %broadcast_multiply_fusion.tiles_ref, bf16[128,128]{1,0:T(8,128)(2,1)S(1)} %copy-done.6, bf16[128,128]{1,0:T(8,128)(2,1)S(1)} %copy-done.7, ...), custom_call_target="tpu_custom_call" | custom-call | tf_op jit(solution)/shard_map/grads/pallas_call | solution.py:204
  54.7 46.8 %all_to_all.10.back_ref = bf16[64,96,128]{2,1,0:T(8,128)(2,1)S(1)} all-to-all(bf16[64,96,128]{2,1,0:T(8,128)(2,1)S(1)} %get-tuple-element.15), channel_id=1, replica_groups=mesh['kv'=64,'tp'=8] {'kv'}, dimensions={0} | all-to-all | bytes 3145728 | tf_op jit(solution)/shard_map/all_to_all | solution.py:220
  101.5 1.8 %settle.1 = (bf16[128,128]{1,0:T(8,128)(2,1)}, bf16[128,128]{1,0:T(8,128)(2,1)}, f32[32,128]{1,0:T(8,128)}) custom-call(bf16[64,96,128]{2,1,0:T(8,128)(2,1)S(1)} %all_to_all.10.back_ref, f32[64,128]{1,0:T(8,128)S(1)} %get-tuple-element.16.ids_ref, f32[128,128]{1,0:T(8,128)S(1)} %get-tuple-element.17.dk_ref, f32[128,128]{1,0:T(8,128)S(1)} %get-tuple-element.18.dv_ref), custom_call_target="tpu_custom_call" | custom-call | tf_op jit(solution)/shard_map/settle/pallas_call | solution.py:221
  (6 shorter events, 0.0 us)
Async XLA Ops:
  0.6 21.0 %copy-start.8 = (f32[2,128]{1,0:T(2,128)S(1)}, f32[2,128]{1,0:T(2,128)}, u32[]{:S(2)}) copy-start(f32[2,128]{1,0:T(2,128)} %param.11) | copy-start | bytes 3076
  0.6 0.8 copy-start
  1.4 0.8 copy-start.2
  2.2 0.7 copy-start.4
  2.9 18.2 %copy-start.5 = (s32[2,256,12]{1,0,2:T(2,128)S(1)}, s32[2,256,12]{1,0,2:T(2,128)}, u32[]{:S(2)}) copy-start(s32[2,256,12]{1,0,2:T(2,128)} %param.12) | copy-start | bytes 73732
  2.9 18.5 %copy-start.9 = (bf16[128,256]{1,0:T(8,128)(2,1)S(1)}, bf16[128,256]{1,0:T(8,128)(2,1)}, u32[]{:S(2)}) copy-start(bf16[128,256]{1,0:T(8,128)(2,1)} %param.13) | copy-start | bytes 196612
  4.4 46.4 %all-to-all-start = ((bf16[64,64,128]{2,1,0:T(8,128)(2,1)}), bf16[64,64,128]{2,1,0:T(8,128)(2,1)S(1)}, u32[]{:S(2)}, u32[]{:S(2)}) async-start(bf16[64,64,128]{2,1,0:T(8,128)(2,1)} %get-tuple-element.13), calls=%async_computation | async-start | bytes 2097152 | tf_op jit(solution)/shard_map/all_to_all | solution.py:187
  21.0 29.9 %copy-start.1 = (bf16[128,128]{1,0:T(8,128)(2,1)S(1)}, bf16[128,128]{1,0:T(8,128)(2,1)}, u32[]{:S(2)}) copy-start(bf16[128,128]{1,0:T(8,128)(2,1)} %k_ref.3) | copy-start | bytes 98308
  21.0 29.9 %copy-start.3 = (bf16[128,128]{1,0:T(8,128)(2,1)S(1)}, bf16[128,128]{1,0:T(8,128)(2,1)}, u32[]{:S(2)}) copy-start(bf16[128,128]{1,0:T(8,128)(2,1)} %v_ref.3) | copy-start | bytes 98308
  21.1 29.9 %copy-start.6 = (bf16[128,128]{1,0:T(8,128)(2,1)S(1)}, bf16[128,128]{1,0:T(8,128)(2,1)}, u32[]{:S(2)}) copy-start(bf16[128,128]{1,0:T(8,128)(2,1)} %q_ref.1) | copy-start | bytes 98308
  21.1 29.9 %copy-start.7 = (bf16[128,128]{1,0:T(8,128)(2,1)S(1)}, bf16[128,128]{1,0:T(8,128)(2,1)}, u32[]{:S(2)}) copy-start(bf16[128,128]{1,0:T(8,128)(2,1)} %g_ref.1) | copy-start | bytes 98308
